TPU v7x, 32 devices: a whole 2x2x4 slice. The times are simulated.
32 devices in a mesh: fs: 4 (over y, x), tp: 8 (over z, core).
Axes of the slice: x: 2, y: 2, z: 4, core: 2. Of those that a mesh axis runs over, the one named last changes fastest.
Arguments:
- value_input: bfloat16 [8192, 2048], P('fs', 'tp'), may hold values from -50 to 50
- value_cotangent: bfloat16 [8192, 512], P('fs'), may hold values from -6 to 6
- value_factor: bfloat16 [512, 128], replicated, may hold values from -10 to 10
- value_master: float32 [512, 2048], P('fs', 'tp'), may hold values from -0.125 to 0.125
- value_first: float32 [128, 2048], P('fs', 'tp'), may hold values from -4 to 4
- value_second: float32 [128, 2048], P('fs', 'tp'), may hold values from 0.01 to 0.2
- mixed_heads: bfloat16 [8192, 1024], P('fs', 'tp'), may hold values from -6 to 6
- output_cotangent: bfloat16 [8192, 2048], P('fs', 'tp'), may hold values from -50 to 50
- output_factor: bfloat16 [1024, 128], replicated, may hold values from -10 to 10
- output_master: float32 [1024, 2048], P('fs', 'tp'), may hold values from -0.1875 to 0.1875
- output_first: float32 [128, 2048], P('fs', 'tp'), may hold values from -4 to 4
- output_second: float32 [128, 2048], P('fs', 'tp'), may hold values from 0.01 to 0.2
Outputs:
- value_step: float32 [512, 2048], P('fs', 'tp')
- value_new_master: float32 [512, 2048], P('fs', 'tp')
- value_copy: bfloat16 [512, 2048], P(None, 'tp')
- value_first_new: float32 [128, 2048], P('fs', 'tp')
- value_second_new: float32 [128, 2048], P('fs', 'tp')
- output_step: float32 [1024, 2048], P('fs', 'tp')
- output_new_master: float32 [1024, 2048], P('fs', 'tp')
- output_copy: bfloat16 [1024, 2048], P(None, 'tp')
- output_first_new: float32 [128, 2048], P('fs', 'tp')
- output_second_new: float32 [128, 2048], P('fs', 'tp')
All inputs are finite; a program needn't handle non-finite values.
Results may differ from a plain program's by a relative error of at most 0.001.
Values may be sent and summed in bfloat16 or wider, within the bound.
A program may use at most 64 MiB of HBM per device.

v0:
```python
import jax
import jax.numpy as jnp
from jax import lax
from jax.sharding import PartitionSpec as P

highest = lax.Precision.HIGHEST


def tokens_exact(left, right):
    return lax.dot_general(
        left, right, (((0,), (0,)), ((), ())), precision=highest, preferred_element_type=jnp.float32
    )


def moment_update(projected, scale, first, second):
    scaled = scale * projected
    first_new = 0.9 * first + 0.1 * scaled
    second_new = 0.95 * second + 0.05 * scaled * scaled
    direction = first_new / (jnp.sqrt(second_new) + 1e-08)
    return (first_new, second_new, direction)


def project_both(value_image, output_image, value_input, output_cotangent, band):
    value_wide = value_input.astype(jnp.float32)
    output_wide = output_cotangent.astype(jnp.float32)
    columns = value_input.shape[1]
    blocks = lax.axis_size("fs") * (2 * band) // (2 * band)
    value_term = tokens_exact(value_image, value_wide).reshape(blocks, band, columns)
    output_term = tokens_exact(output_image, output_wide).reshape(blocks, band, columns)
    paired = lax.psum_scatter(
        jnp.stack([value_term, output_term], axis=1).reshape(
            lax.axis_size("fs") * (2 * band), columns
        ),
        "fs",
        scatter_dimension=0,
        tiled=True,
    )
    return (paired[:band], paired[band:])


def on_device(
    value_input,
    value_cotangent,
    value_factor,
    value_master,
    value_first,
    value_second,
    mixed_heads,
    output_cotangent,
    output_factor,
    output_master,
    output_first,
    output_second,
):
    fs_count = lax.axis_size("fs")
    fs_place = lax.axis_index("fs")
    rank = value_factor.shape[1]
    band = rank // fs_count
    columns = value_input.shape[1]
    value_rows = value_master.shape[0]
    output_rows = output_master.shape[0]
    value_block = lax.dynamic_slice_in_dim(
        value_factor, fs_place * value_rows, value_rows, 0
    ).astype(jnp.float32)
    output_block = lax.dynamic_slice_in_dim(
        output_factor, fs_place * output_rows, output_rows, 0
    ).astype(jnp.float32)
    value_image = jnp.dot(value_cotangent, value_factor, preferred_element_type=jnp.float32)
    heads_whole = lax.all_gather(mixed_heads, "tp", axis=1, tiled=True)
    output_image = jnp.dot(heads_whole, output_factor, preferred_element_type=jnp.float32)
    value_proj, output_proj = project_both(
        value_image, output_image, value_input, output_cotangent, band
    )
    total_count = rank * columns * lax.axis_size("tp")
    value_square, output_square = lax.psum(
        (jnp.sum(value_proj * value_proj), jnp.sum(output_proj * output_proj)), ("fs", "tp")
    )
    value_scale = lax.rsqrt(value_square / total_count + 1e-06)
    output_scale = lax.rsqrt(output_square / total_count + 1e-06)
    value_first_new, value_second_new, value_dir = moment_update(
        value_proj, value_scale, value_first, value_second
    )
    output_first_new, output_second_new, output_dir = moment_update(
        output_proj, output_scale, output_first, output_second
    )
    value_dir_all, output_dir_all = (
        lax.all_gather(value_dir, "fs", axis=0, tiled=True),
        lax.all_gather(output_dir, "fs", axis=0, tiled=True),
    )
    value_step = jnp.dot(
        value_block, value_dir_all, precision=highest, preferred_element_type=jnp.float32
    )
    output_step = jnp.dot(
        output_block, output_dir_all, precision=highest, preferred_element_type=jnp.float32
    )
    value_new = value_master - 0.002 * value_step
    output_new = output_master - 0.002 * output_step
    value_copy, output_copy = (
        lax.all_gather(value_new.astype(jnp.bfloat16), "fs", axis=0, tiled=True),
        lax.all_gather(output_new.astype(jnp.bfloat16), "fs", axis=0, tiled=True),
    )
    return (
        value_step,
        value_new,
        value_copy,
        value_first_new,
        value_second_new,
        output_step,
        output_new,
        output_copy,
        output_first_new,
        output_second_new,
    )


def solution(mesh):
    in_specs = (
        P("fs", "tp"),
        P("fs", None),
        P(),
        P("fs", "tp"),
        P("fs", "tp"),
        P("fs", "tp"),
        P("fs", "tp"),
        P("fs", "tp"),
        P(),
        P("fs", "tp"),
        P("fs", "tp"),
        P("fs", "tp"),
    )
    out_specs = (
        P("fs", "tp"),
        P("fs", "tp"),
        P(None, "tp"),
        P("fs", "tp"),
        P("fs", "tp"),
        P("fs", "tp"),
        P("fs", "tp"),
        P(None, "tp"),
        P("fs", "tp"),
        P("fs", "tp"),
    )
    return jax.shard_map(
        on_device, mesh=mesh, in_specs=in_specs, out_specs=out_specs, check_vma=False
    )
```

profile of v0, /device:TPU:0, one launch (start us, length us, event | category | flops | bytes accessed | tf_op | source)
XLA Modules:
  0.0 180.0 jit_solution(13130348635020009282)
XLA Ops:
  7.2 0.0 copy-start
  7.2 0.0 copy-start.1
  7.2 0.0 copy-start.3
  7.2 0.0 all-gather.2.cloned.1.call-start
  7.3 0.7 all-gather.2.cloned.1.call-update
  7.9 0.0 reduce-scatter.2.cloned.1.call-start
  8.0 0.8 copy-done
  8.8 1.6 fusion.12
  10.4 0.0 copy-done.1
  10.4 1.0 fusion.13
  11.4 0.0 copy-start.2
  11.4 48.8 %all-gather.2.cloned.1.call-done = bf16[2048,1024]{1,0:T(8,128)(2,1)} async-done(((bf16[2048,128]{1,0:T(8,128)(2,1)}), bf16[2048,1024]{1,0:T(8,128)(2,1)}) %all-gather.2.cloned.1.call-update) | async-done | bytes 4194320 | tf_op jit(solution)/shard_map/all_gather | solution.py:69
  60.2 0.0 copy-done.3
  60.2 3.5 %fusion.14 = f32[2048,128]{1,0:T(8,128)S(1)} fusion(bf16[2048,1024]{1,0:T(8,128)(2,1)} %all-gather.2.cloned.1.call-done, bf16[1024,128]{1,0:T(8,128)(2,1)S(1)} %copy-done.3), kind=kOutput, calls=%fused_computation.25 | convolution fusion | flops 536870912 | bytes 5505024 | tf_op jit(solution)/shard_map/dot_general | solution.py:70
  63.7 0.0 copy-done.2
  63.7 1.0 fusion.15
  64.7 0.7 copy.22
  65.5 0.0 reduce-scatter.2.cloned.1.call-update
  65.5 22.7 %reduce-scatter.2.cloned.1.call-done = f32[64,256]{1,0:T(8,128)} async-done(((f32[256,256]{1,0:T(8,128)}), f32[64,256]{1,0:T(8,128)}) %reduce-scatter.2.cloned.1.call-update) | async-done | bytes 65552 | tf_op jit(solution)/shard_map/reduce_scatter | solution.py:30
  88.2 1.4 multiply_reduce_fusion
  89.6 39.5 %all-reduce = (f32[]{:T(128)}, f32[]{:T(128)}) all-reduce(f32[]{:T(128)} %get-tuple-element.11, f32[]{:T(128)} %get-tuple-element.10), channel_id=1, replica_groups=mesh['fs'=4,'tp'=8] {'fs','tp'}, use_global_device_ids=true, to_apply=%region_2.0 | all-reduce | flops 2 | bytes 16 | tf_op jit(solution)/shard_map/psum | solution.py:75
  130.5 1.5 add_divide_fusion
  132.0 9.4 %all_gather.18 = f32[128,256]{1,0:T(8,128)S(1)} all-gather(f32[32,256]{1,0:T(8,128)S(1)} %get-tuple-element.16), channel_id=1, replica_groups=mesh['fs'=4,'tp'=8] {'fs'}, dimensions={0}, use_global_device_ids=true | all-gather | bytes 163840 | tf_op jit(solution)/shard_map/all_gather | solution.py:88
  141.4 2.0 %fusion.8 = (bf16[256,256]{1,0:T(8,128)(2,1)S(1)}, f32[256,256]{1,0:T(8,128)}, f32[256,256]{1,0:T(8,128)}) fusion(f32[256,256]{1,0:T(8,128)} %param.21, f32[128,256]{1,0:T(8,128)S(1)} %all_gather.18, bf16[1024,128]{1,0:T(8,128)(2,1)S(1)} %copy-done.3, s32[]{:T(128)S(6)} %select_n.7), kind=kOutput, calls=%fused_computation.21 | convolution fusion | flops 100859904 | bytes 1114116 | tf_op jit(solution)/shard_map/dot_general | solution.py:93
  143.4 10.0 %all_gather.19 = bf16[1024,256]{1,0:T(8,128)(2,1)S(1)} all-gather(bf16[256,256]{1,0:T(8,128)(2,1)S(1)} %get-tuple-element.14), channel_id=1, replica_groups=mesh['fs'=4,'tp'=8] {'fs'}, dimensions={0}, use_global_device_ids=true | all-gather | bytes 655360 | tf_op jit(solution)/shard_map/all_gather | solution.py:100
  153.4 7.7 %all_gather.16 = f32[128,256]{1,0:T(8,128)S(1)} all-gather(f32[32,256]{1,0:T(8,128)S(1)} %get-tuple-element.24), channel_id=1, replica_groups=mesh['fs'=4,'tp'=8] {'fs'}, dimensions={0}, use_global_device_ids=true | all-gather | bytes 163840 | tf_op jit(solution)/shard_map/all_gather | solution.py:87
  161.0 1.8 %fusion.10 = (bf16[128,256]{1,0:T(8,128)(2,1)S(1)}, f32[128,256]{1,0:T(8,128)}, f32[128,256]{1,0:T(8,128)}) fusion(f32[128,256]{1,0:T(8,128)} %param.15, f32[128,256]{1,0:T(8,128)S(1)} %all_gather.16, bf16[512,128]{1,0:T(8,128)(2,1)} %param.14, s32[]{:T(128)S(6)} %select_n.6), kind=kOutput, calls=%fused_computation.22 | convolution fusion | flops 50429952 | bytes 622596 | tf_op jit(solution)/shard_map/dot_general | solution.py:90
  162.9 8.8 %all_gather.17 = bf16[512,256]{1,0:T(8,128)(2,1)S(1)} all-gather(bf16[128,256]{1,0:T(8,128)(2,1)S(1)} %get-tuple-element.19), channel_id=1, replica_groups=mesh['fs'=4,'tp'=8] {'fs'}, dimensions={0}, use_global_device_ids=true | all-gather | bytes 327680 | tf_op jit(solution)/shard_map/all_gather | solution.py:99
  171.6 0.7 copy.25
  172.3 0.8 copy.26
  (1 shorter events, 0.0 us)
Async XLA Ops:
  7.2 1.6 copy-start
  7.2 3.2 %copy-start.1 = (bf16[2048,256]{1,0:T(8,128)(2,1)S(1)}, bf16[2048,256]{1,0:T(8,128)(2,1)}, u32[]{:S(2)}) copy-start(bf16[2048,256]{1,0:T(8,128)(2,1)} %param.12) | copy-start | bytes 3145732
  7.2 53.0 %copy-start.3 = (bf16[1024,128]{1,0:T(8,128)(2,1)S(1)}, bf16[1024,128]{1,0:T(8,128)(2,1)}, u32[]{:S(2)}) copy-start(bf16[1024,128]{1,0:T(8,128)(2,1)} %param.20) | copy-start | bytes 786436
  7.2 53.0 %all-gather.2.cloned.1.call-start = ((), (), s32[]{:S(2)}) async-start(), calls=%async_computation.1 | async-start | bytes 4718592 | tf_op jit(solution)/shard_map/all_gather | solution.py:69
  7.9 80.2 %reduce-scatter.2.cloned.1.call-start = ((), (), s32[]{:S(2)}) async-start(), calls=%async_computation.2 | async-start | bytes 327680 | tf_op jit(solution)/shard_map/reduce_scatter | solution.py:30
  11.4 52.3 %copy-start.2 = (bf16[2048,256]{1,0:T(8,128)(2,1)S(1)}, bf16[2048,256]{1,0:T(8,128)(2,1)}, u32[]{:S(2)}) copy-start(bf16[2048,256]{1,0:T(8,128)(2,1)} %param.19) | copy-start | bytes 3145732
Sparse Core Ops, SparseCore 0:
  9.6 50.5 all-gather.1
  65.6 22.5 reduce-scatter.1
where the time goes:
time: 180 us
  blocking collectives  75.3 us (42%)
  waiting for transfers between devices  72.2 us (40%)
  between operations  15.5 us (9%)
  matrix products  10.9 us (6%)
  local copies, waits for them, and re-layouts  3.02 us (2%)
  other arithmetic  2.93 us (2%)
    all_gather x1, waiting for transfers between devices, on_device(): heads_whole = lax.all_gather(mixed_heads, 'tp', axis=1, tiled=True)  48.8 us
    psum x1, blocking collectives, on_device(): lax.psum((jnp.sum(value_proj * value_proj), jnp.sum(output_proj * output_...  39.5 us
    reduce_scatter x1, waiting for transfers between devices, project_both(): lax.psum_scatter(jnp.stack([value_term, output_term], axis=1).reshape(lax...  22.7 us
    all_gather x1, blocking collectives, on_device(): lax.all_gather(output_new.astype(jnp.bfloat16), 'fs', axis=0, tiled=True)  9.99 us
    all_gather x1, blocking collectives, on_device(): lax.all_gather(output_dir, 'fs', axis=0, tiled=True)  9.39 us
    all_gather x1, blocking collectives, on_device(): lax.all_gather(value_new.astype(jnp.bfloat16), 'fs', axis=0, tiled=True)  8.76 us
    all_gather x1, blocking collectives, on_device(): lax.all_gather(value_dir, 'fs', axis=0, tiled=True)  7.66 us
  transfers between devices with their start and end apart: 2, of which 2 were waited for; matrix products, arithmetic and copies ran while one was open for 1% of the time, Pallas kernels for 0%

commit v1 on v0

v1 whole, which is shorter than its diff:
```python
import functools

import jax
import jax.numpy as jnp
from jax import lax
from jax.experimental import pallas as pl
from jax.experimental.pallas import tpu as pltpu
from jax.sharding import PartitionSpec as P

MESH = pl.DeviceIdType.MESH
ANY = pl.BlockSpec(memory_space=pl.ANY)
VMEM = pl.BlockSpec(memory_space=pltpu.VMEM)
BF16 = jnp.bfloat16
F32 = jnp.float32


def split(wide, axis):
    high = wide.astype(BF16)
    low = (wide - high.astype(F32)).astype(BF16)
    return jnp.concatenate([high, low], axis=axis)


def gather_kernel(
    fs, tp, pair,
    vin, vcot, vfac, vmas, vm1, vm2, heads, ocot, ofac, omas, om1, om2,
    v_all, o_all, v1_all, v2_all, o1_all, o2_all, vm_all, om_all, totals,
    vin_v, vcot_v, heads_v, ocot_v, v1_v, v2_v, o1_v, o2_v, vm_v, om_v,
    heads_in, images, partial, partial_in, band_v, first_sums, second_sums,
    load_sem, own_sem, put_sem, heads_send, heads_recv, image_send, image_recv, relay_send,
    rs_send, rs_recv, all_send, all_recv, s1_send, s1_recv, s2_send, s2_recv, pre_send, pre_recv,
):
    f = lax.axis_index("fs")
    t = lax.axis_index("tp")
    rank = vfac.shape[1]
    band = rank // fs
    tokens, width = heads.shape
    block = tokens // tp
    columns = vin.shape[1]

    def fs_peer(j):
        return lax.rem(f + j, fs)

    def tp_peer(j):
        return lax.rem(t + j, tp)

    sources = (heads, om1, om2, vm1, vm2, vcot, vin, omas, vmas, ocot)
    places = (heads_v, o1_v, o2_v, v1_v, v2_v, vcot_v, vin_v, om_v, vm_v, ocot_v)
    loads = [
        pltpu.make_async_copy(a, b, load_sem.at[i]) for i, (a, b) in enumerate(zip(sources, places))
    ]
    for load in loads:
        load.start()

    barrier = pltpu.get_barrier_semaphore()
    for j in range(1, tp):
        pl.semaphore_signal(barrier, inc=1, device_id={"tp": tp_peer(j)}, device_id_type=MESH)
    for j in range(1, fs):
        pl.semaphore_signal(barrier, inc=1, device_id={"fs": fs_peer(j)}, device_id_type=MESH)
    pl.semaphore_wait(barrier, tp + fs - 2)

    sent = []

    def send(src, dst, send_sem, recv_sem, where):
        copy = pltpu.make_async_remote_copy(
            src_ref=src, dst_ref=dst, send_sem=send_sem, recv_sem=recv_sem,
            device_id=where, device_id_type=MESH,
        )
        copy.start()
        sent.append(copy)

    def landed(dst, send_sem, recv_sem, where):
        pltpu.make_async_remote_copy(
            src_ref=dst, dst_ref=dst, send_sem=send_sem, recv_sem=recv_sem,
            device_id=where, device_id_type=MESH,
        ).wait_recv()

    loads[0].wait()
    for j in range(1, tp):
        d = tp_peer(j)
        send(
            heads_v.at[pl.ds(pl.multiple_of(d * block, block), block)], heads_in.at[t],
            heads_send.at[j], heads_recv.at[t], {"tp": d},
        )
    own_heads = pltpu.make_async_copy(
        heads_v.at[pl.ds(pl.multiple_of(t * block, block), block)], heads_in.at[t], own_sem
    )
    own_heads.start()

    puts = []

    def prefetch(i, load, local, whole):
        load.wait()
        rows = local.shape[0]
        here = whole.at[pl.ds(pl.multiple_of(f * rows, rows), rows)]
        for j in range(1, fs):
            d = fs_peer(j)
            send(local, here, pre_send.at[i, j], pre_recv.at[i, f], {"fs": d})
        put = pltpu.make_async_copy(local, here, put_sem.at[i])
        put.start()
        puts.append(put)

    prefetch(0, loads[1], o1_v, o1_all)
    prefetch(1, loads[2], o2_v, o2_all)
    prefetch(2, loads[3], v1_v, v1_all)
    prefetch(3, loads[4], v2_v, v2_all)

    loads[5].wait()
    loads[6].wait()
    total = jnp.zeros((2 * rank, columns), F32)
    step = 256 if tokens % 256 == 0 else tokens
    for i in range(tokens // step):
        rows = pl.ds(i * step, step)
        image = jnp.dot(vcot_v[rows, :], vfac[...], preferred_element_type=F32)
        total = total + lax.dot_general(
            split(image, 1), vin_v[rows, :], (((0,), (0,)), ((), ())), preferred_element_type=F32
        )

    def scatter(k, total):
        partial[k] = (total[:rank] + total[rank:]).reshape(fs, band, columns)
        for j in range(1, fs):
            d = fs_peer(j)
            send(partial.at[k, d], partial_in.at[k, f], rs_send.at[k, j], rs_recv.at[k, f], {"fs": d})

    def reduce(k, whole):
        mine = partial[k, f]
        for j in range(1, fs):
            d = fs_peer(j)
            landed(partial_in.at[k, d], rs_send.at[k, j], rs_recv.at[k, d], {"fs": d})
            mine = mine + partial_in[k, d]
        band_v[k] = mine
        first_sums[k, f] = jnp.full((8, 128), jnp.sum(mine * mine), F32)
        for j in range(1, fs):
            d = fs_peer(j)
            send(first_sums.at[k, f], first_sums.at[k, f], s1_send.at[k, j], s1_recv.at[k, f], {"fs": d})
        for j in range(1, fs):
            d = fs_peer(j)
            send(band_v.at[k], whole.at[f], all_send.at[k, j], all_recv.at[k, f], {"fs": d})
        put = pltpu.make_async_copy(band_v.at[k], whole.at[f], put_sem.at[6 + k])
        put.start()
        puts.append(put)

    def sums_on(k):
        mine = first_sums[k, f]
        for j in range(1, fs):
            d = fs_peer(j)
            landed(first_sums.at[k, d], s1_send.at[k, j], s1_recv.at[k, d], {"fs": d})
            mine = mine + first_sums[k, d]
        second_sums[k, t] = mine
        for j in range(1, tp):
            d = tp_peer(j)
            send(second_sums.at[k, t], second_sums.at[k, t], s2_send.at[k, j], s2_recv.at[k, t], {"tp": d})

    def sums_end(k):
        mine = second_sums[k, t]
        for j in range(1, tp):
            d = tp_peer(j)
            landed(second_sums.at[k, d], s2_send.at[k, j], s2_recv.at[k, d], {"tp": d})
            mine = mine + second_sums[k, d]
        totals[k] = mine

    scatter(0, total)
    prefetch(4, loads[7], om_v, om_all)
    prefetch(5, loads[8], vm_v, vm_all)

    own_heads.wait()

    def image_term(s):
        return jnp.dot(
            heads_in[s], ofac[pl.ds(pl.multiple_of(s * width, width), width), :],
            preferred_element_type=F32,
        )

    image = image_term(t)
    for j in range(1, tp):
        d = tp_peer(j)
        landed(heads_in.at[d], heads_send.at[j], heads_recv.at[d], {"tp": d})
        image = image + image_term(d)
    images[t] = image.T

    chip = t // pair
    core = t % pair
    chips = tp // pair

    def give(d, j):
        send(images.at[t], images.at[t], image_send.at[j], image_recv.at[t], {"tp": d})

    for j in range(1, chips):
        give(lax.rem(chip + j, chips) * pair + core, j - 1)
    for j in range(1, pair):
        give(chip * pair + lax.rem(core + j, pair), chips - 2 + j)

    loads[9].wait()

    def term(s):
        return jnp.dot(
            split(images[s], 0), ocot_v[pl.ds(pl.multiple_of(s * block, block), block), :],
            preferred_element_type=F32,
        )

    total = term(t)
    reduce(0, v_all)

    def arrived(s):
        landed(images.at[s], image_send.at[0], image_recv.at[s], {"tp": s})

    for j in range(1, pair):
        s = chip * pair + lax.rem(core + j, pair)
        arrived(s)
        total = total + term(s)
    for j in range(1, chips):
        s = lax.rem(chip + j, chips) * pair + core
        arrived(s)
        for i in range(1, pair):
            send(
                images.at[s], images.at[s], relay_send.at[(j - 1) * (pair - 1) + i - 1],
                image_recv.at[s], {"tp": chip * pair + lax.rem(core + i, pair)},
            )
        total = total + term(s)
    for j in range(1, chips):
        for i in range(1, pair):
            s = lax.rem(chip + j, chips) * pair + lax.rem(core + i, pair)
            arrived(s)
            total = total + term(s)

    scatter(1, total)
    sums_on(0)
    reduce(1, o_all)
    sums_on(1)
    sums_end(0)
    sums_end(1)

    for k, whole in ((0, v_all), (1, o_all)):
        for j in range(1, fs):
            d = fs_peer(j)
            landed(whole.at[d], all_send.at[k, j], all_recv.at[k, d], {"fs": d})
    for i, (local, whole) in enumerate(
        ((o1_v, o1_all), (o2_v, o2_all), (v1_v, v1_all), (v2_v, v2_all), (om_v, om_all), (vm_v, vm_all))
    ):
        rows = local.shape[0]
        for j in range(1, fs):
            d = fs_peer(j)
            there = whole.at[pl.ds(pl.multiple_of(d * rows, rows), rows)]
            landed(there, pre_send.at[i, j], pre_recv.at[i, d], {"fs": d})
    for copy in sent:
        copy.wait_send()
    for put in puts:
        put.wait()


def finish_kernel(
    fs, tp,
    v_all, o_all, v1_all, v2_all, o1_all, o2_all, vm_all, om_all, totals, vfac, ofac,
    v_step, v_new, v_copy, v_first, v_second, o_step, o_new, o_copy, o_first, o_second,
):
    f = lax.axis_index("fs")

    def one(k, proj, first, second, master, factor, step_out, new_out, copy_out, first_out, second_out):
        rank, columns = proj.shape
        scale = lax.rsqrt(totals[k, 0:1, 0:1] / (rank * columns * tp) + 1e-06)

        def moments(rows):
            scaled = scale * proj[rows, :]
            first_new = 0.9 * first[rows, :] + 0.1 * scaled
            second_new = 0.95 * second[rows, :] + 0.05 * scaled * scaled
            return first_new, second_new

        band = rank // fs
        first_own, second_own = moments(pl.ds(pl.multiple_of(f * band, band), band))
        first_out[...] = first_own
        second_out[...] = second_own
        first_new, second_new = moments(pl.ds(0, rank))
        direction = split(first_new / (jnp.sqrt(second_new) + 1e-08), 0)

        def step_of(rows):
            left = factor[rows, :]
            return jnp.dot(
                jnp.concatenate([left, left], axis=1), direction, preferred_element_type=F32
            )

        count = step_out.shape[0]
        own = pl.ds(pl.multiple_of(f * count, count), count)
        step = step_of(own)
        step_out[...] = step
        new_out[...] = master[own, :] - 0.002 * step
        for i in range(fs):
            rows = pl.ds(i * count, count)
            copy_out[rows, :] = (master[rows, :] - 0.002 * step_of(rows)).astype(BF16)

    one(0, v_all, v1_all, v2_all, vm_all, vfac, v_step, v_new, v_copy, v_first, v_second)
    one(1, o_all, o1_all, o2_all, om_all, ofac, o_step, o_new, o_copy, o_first, o_second)


def on_device(vin, vcot, vfac, vmas, vm1, vm2, heads, ocot, ofac, omas, om1, om2):
    fs = lax.axis_size("fs")
    tp = lax.axis_size("tp")
    pair = 2 if tp % 2 == 0 else 1
    rank = vfac.shape[1]
    band = rank // fs
    columns = vin.shape[1]
    tokens, width = heads.shape
    block = tokens // tp

    def like(array):
        return pltpu.VMEM(array.shape, array.dtype)

    def shape(*dims):
        return jax.ShapeDtypeStruct(dims, F32)

    dma = pltpu.SemaphoreType.DMA
    gathered = pl.pallas_call(
        functools.partial(gather_kernel, fs, tp, pair),
        out_shape=(
            shape(fs, band, columns), shape(fs, band, columns),
            shape(rank, columns), shape(rank, columns), shape(rank, columns), shape(rank, columns),
            shape(fs * vmas.shape[0], columns), shape(fs * omas.shape[0], columns),
            shape(2, 8, 128),
        ),
        in_specs=[ANY, ANY, VMEM, ANY, ANY, ANY, ANY, ANY, VMEM, ANY, ANY, ANY],
        out_specs=(ANY,) * 8 + (VMEM,),
        scratch_shapes=[
            like(vin), like(vcot), like(heads), like(ocot), like(vm1), like(vm2), like(om1), like(om2),
            like(vmas), like(omas),
            pltpu.VMEM((tp, block, width), BF16),
            pltpu.VMEM((tp, rank, block), F32),
            pltpu.VMEM((2, fs, band, columns), F32),
            pltpu.VMEM((2, fs, band, columns), F32),
            pltpu.VMEM((2, band, columns), F32),
            pltpu.VMEM((2, fs, 8, 128), F32),
            pltpu.VMEM((2, tp, 8, 128), F32),
            dma((10,)), dma, dma((8,)), dma((tp,)), dma((tp,)), dma((tp,)), dma((tp,)), dma((tp,)),
            dma((2, fs)), dma((2, fs)), dma((2, fs)), dma((2, fs)), dma((2, fs)), dma((2, fs)),
            dma((2, tp)), dma((2, tp)), dma((6, fs)), dma((6, fs)),
        ],
        compiler_params=pltpu.CompilerParams(
            collective_id=0, has_side_effects=True, vmem_limit_bytes=40 * 1024 * 1024
        ),
    )(vin, vcot, vfac, vmas, vm1, vm2, heads, ocot, ofac, omas, om1, om2)
    v_all, o_all, v1_all, v2_all, o1_all, o2_all, vm_all, om_all, totals = gathered
    v_all = v_all.reshape(rank, columns)
    o_all = o_all.reshape(rank, columns)

    def out(array, rows, kind=F32):
        return jax.ShapeDtypeStruct((rows, columns), kind)

    return pl.pallas_call(
        functools.partial(finish_kernel, fs, tp),
        out_shape=(
            out(vmas, vmas.shape[0]), out(vmas, vmas.shape[0]), out(vmas, fs * vmas.shape[0], BF16),
            out(vm1, band), out(vm1, band),
            out(omas, omas.shape[0]), out(omas, omas.shape[0]), out(omas, fs * omas.shape[0], BF16),
            out(om1, band), out(om1, band),
        ),
        in_specs=[VMEM] * 11,
        out_specs=(VMEM,) * 10,
        compiler_params=pltpu.CompilerParams(vmem_limit_bytes=40 * 1024 * 1024),
    )(v_all, o_all, v1_all, v2_all, o1_all, o2_all, vm_all, om_all, totals, vfac, ofac)


def solution(mesh):
    both = P("fs", "tp")
    in_specs = (both, P("fs", None), P(), both, both, both, both, both, P(), both, both, both)
    out_specs = (
        both, both, P(None, "tp"), both, both, both, both, P(None, "tp"), both, both,
    )
    return jax.shard_map(
        on_device, mesh=mesh, in_specs=in_specs, out_specs=out_specs, check_vma=False
    )
```

time: 180 us -> 61 us (0.34)
  blocking collectives: 75.3 us -> 0 us
  waiting for transfers between devices: 72.2 us -> 0 us
  Pallas kernels: 0 us -> 47.8 us
  between operations: 15.5 us -> 0.68 us
  matrix products: 10.9 us -> 0 us
  local copies, waits for them, and re-layouts: 3.02 us -> 11.8 us
  other arithmetic: 2.93 us -> 0 us
    all_gather x1 -> x0, waiting for transfers between devices: 48.8 us -> none  [on_device(): heads_whole = lax.all_gather(mixed_heads, 'tp', axis=1, tiled=True)]
    pallas_call x0 -> x2, Pallas kernels: none -> 47.8 us  [the longest x1 46.3 us: on_device(): pl.pallas_call(functools.partial(gather_kernel, fs, tp, pair), out_shape=...]
    psum x1 -> x0, blocking collectives: 39.5 us -> none  [on_device(): lax.psum((jnp.sum(value_proj * value_proj), jnp.sum(output_proj * output_...]
    all_gather x4 -> x0, blocking collectives: 35.8 us -> none  [the longest x1 9.99 us: on_device(): lax.all_gather(output_new.astype(jnp.bfloat16), 'fs', axis=0, tiled=True)]
    reduce_scatter x1 -> x0, waiting for transfers between devices: 22.7 us -> none  [project_both(): lax.psum_scatter(jnp.stack([value_term, output_term], axis=1).reshape(lax...]
    dot_general x6 -> x0, matrix products: 10.9 us -> none  [the longest x1 3.46 us: on_device(): jnp.dot(heads_whole, output_factor, preferred_element_type=jnp.float32)]
    unnamed x10 -> x24, local copies, waits for them, and re-layouts: 2.3 us -> 11.8 us
  transfers between devices with their start and end apart: 2 -> 0, of which waited for: 2 -> 0; matrix products, arithmetic and copies ran while one was open for 1% -> 0% of each run, Pallas kernels for 0% -> 0%
where the time goes in v1:
time: 61 us; the launch traced here: 60.3 us
  Pallas kernels  47.8 us (78%)
  local copies, waits for them, and re-layouts  11.8 us (19%)
  between operations  0.68 us (1%)
    pallas_call x1, Pallas kernels, on_device(): pl.pallas_call(functools.partial(gather_kernel, fs, tp, pair), out_shape=...  46.3 us
    unnamed x24, local copies, waits for them, and re-layouts  11.8 us
    pallas_call x1, Pallas kernels, on_device(): pl.pallas_call(functools.partial(finish_kernel, fs, tp), out_shape=(out(v...  1.51 us

profile of v1, /device:TPU:0, one launch (start us, length us, event | category | flops | bytes accessed | tf_op | source)
XLA Modules:
  0.0 60.3 jit_solution(13711578320870535822)
XLA Ops:
  0.6 0.0 copy-start
  0.7 1.6 %copy-done = bf16[2048,512]{1,0:T(8,128)(2,1)S(1)} copy-done((bf16[2048,512]{1,0:T(8,128)(2,1)S(1)}, bf16[2048,512]{1,0:T(8,128)(2,1)}, u32[]{:S(2)}) %copy-start) | copy-done | bytes 2097176
  2.2 0.0 copy-start.1
  2.2 1.2 %copy-done.1 = bf16[2048,256]{1,0:T(8,128)(2,1)S(1)} copy-done((bf16[2048,256]{1,0:T(8,128)(2,1)S(1)}, bf16[2048,256]{1,0:T(8,128)(2,1)}, u32[]{:S(2)}) %copy-start.1) | copy-done | bytes 1048600
  3.5 0.0 copy-start.2
  3.5 1.2 %copy-done.2 = bf16[2048,256]{1,0:T(8,128)(2,1)S(1)} copy-done((bf16[2048,256]{1,0:T(8,128)(2,1)S(1)}, bf16[2048,256]{1,0:T(8,128)(2,1)}, u32[]{:S(2)}) %copy-start.2) | copy-done | bytes 1048600
  4.7 0.0 copy-start.3
  4.7 0.9 %copy-done.3 = bf16[1024,128]{1,0:T(8,128)(2,1)S(1)} copy-done((bf16[1024,128]{1,0:T(8,128)(2,1)S(1)}, bf16[1024,128]{1,0:T(8,128)(2,1)}, u32[]{:S(2)}) %copy-start.3) | copy-done | bytes 262168
  5.6 0.0 copy-start.4
  5.6 1.0 %copy-done.4 = bf16[2048,128]{1,0:T(8,128)(2,1)S(1)} copy-done((bf16[2048,128]{1,0:T(8,128)(2,1)S(1)}, bf16[2048,128]{1,0:T(8,128)(2,1)}, u32[]{:S(2)}) %copy-start.4) | copy-done | bytes 524312
  6.7 0.0 copy-start.5
  6.7 0.9 %copy-done.5 = bf16[512,128]{1,0:T(8,128)(2,1)S(1)} copy-done((bf16[512,128]{1,0:T(8,128)(2,1)S(1)}, bf16[512,128]{1,0:T(8,128)(2,1)}, u32[]{:S(2)}) %copy-start.5) | copy-done | bytes 131096
  7.6 0.0 copy-start.6
  7.6 0.9 %copy-done.6 = f32[256,256]{1,0:T(8,128)S(1)} copy-done((f32[256,256]{1,0:T(8,128)S(1)}, f32[256,256]{1,0:T(8,128)}, u32[]{:S(2)}) %copy-start.6) | copy-done | bytes 262168
  8.5 0.0 copy-start.7
  8.5 0.9 %copy-done.7 = f32[128,256]{1,0:T(8,128)S(1)} copy-done((f32[128,256]{1,0:T(8,128)S(1)}, f32[128,256]{1,0:T(8,128)}, u32[]{:S(2)}) %copy-start.7) | copy-done | bytes 131096
  9.4 0.0 copy-start.8
  9.4 0.8 %copy-done.8 = f32[32,256]{1,0:T(8,128)S(1)} copy-done((f32[32,256]{1,0:T(8,128)S(1)}, f32[32,256]{1,0:T(8,128)}, u32[]{:S(2)}) %copy-start.8) | copy-done | bytes 32792
  10.2 0.0 copy-start.9
  10.2 0.8 %copy-done.9 = f32[32,256]{1,0:T(8,128)S(1)} copy-done((f32[32,256]{1,0:T(8,128)S(1)}, f32[32,256]{1,0:T(8,128)}, u32[]{:S(2)}) %copy-start.9) | copy-done | bytes 32792
  11.0 0.0 copy-start.10
  11.0 0.8 %copy-done.10 = f32[32,256]{1,0:T(8,128)S(1)} copy-done((f32[32,256]{1,0:T(8,128)S(1)}, f32[32,256]{1,0:T(8,128)}, u32[]{:S(2)}) %copy-start.10) | copy-done | bytes 32792
  11.7 0.0 copy-start.11
  11.7 0.8 %copy-done.11 = f32[32,256]{1,0:T(8,128)S(1)} copy-done((f32[32,256]{1,0:T(8,128)S(1)}, f32[32,256]{1,0:T(8,128)}, u32[]{:S(2)}) %copy-start.11) | copy-done | bytes 32792
  12.5 46.3 %shard_map.195 = (f32[4,32,256]{2,1,0:T(8,128)S(1)}, f32[4,32,256]{2,1,0:T(8,128)S(1)}, f32[128,256]{1,0:T(8,128)S(1)}, f32[128,256]{1,0:T(8,128)S(1)}, f32[128,...) custom-call(bf16[2048,256]{1,0:T(8,128)(2,1)S(1)} %copy-done.1, ...), custom_call_target="tpu_custom_call" | custom-call | tf_op jit(solution)/shard_map/pallas_call | solution.py:310
  58.8 1.5 %shard_map.196 = (f32[128,256]{1,0:T(8,128)}, f32[128,256]{1,0:T(8,128)}, bf16[512,256]{1,0:T(8,128)(2,1)}, f32[32,256]{1,0:T(8,128)}, f32[32,256]{1,0:T(8,128)}...) custom-call(f32[128,256]{1,0:T(8,128)S(1)} %bitcast.2, ...), custom_call_target="tpu_custom_call" | custom-call | tf_op jit(solution)/shard_map/pallas_call | solution.py:345
Async XLA Ops:
  0.6 1.6 %copy-start = (bf16[2048,512]{1,0:T(8,128)(2,1)S(1)}, bf16[2048,512]{1,0:T(8,128)(2,1)}, u32[]{:S(2)}) copy-start(bf16[2048,512]{1,0:T(8,128)(2,1)} %vcot.1) | copy-start | bytes 6291460
  2.2 1.2 %copy-start.1 = (bf16[2048,256]{1,0:T(8,128)(2,1)S(1)}, bf16[2048,256]{1,0:T(8,128)(2,1)}, u32[]{:S(2)}) copy-start(bf16[2048,256]{1,0:T(8,128)(2,1)} %vin.1) | copy-start | bytes 3145732
  3.5 1.2 %copy-start.2 = (bf16[2048,256]{1,0:T(8,128)(2,1)S(1)}, bf16[2048,256]{1,0:T(8,128)(2,1)}, u32[]{:S(2)}) copy-start(bf16[2048,256]{1,0:T(8,128)(2,1)} %ocot.1) | copy-start | bytes 3145732
  4.7 0.9 %copy-start.3 = (bf16[1024,128]{1,0:T(8,128)(2,1)S(1)}, bf16[1024,128]{1,0:T(8,128)(2,1)}, u32[]{:S(2)}) copy-start(bf16[1024,128]{1,0:T(8,128)(2,1)} %ofac.3) | copy-start | bytes 786436
  5.6 1.0 %copy-start.4 = (bf16[2048,128]{1,0:T(8,128)(2,1)S(1)}, bf16[2048,128]{1,0:T(8,128)(2,1)}, u32[]{:S(2)}) copy-start(bf16[2048,128]{1,0:T(8,128)(2,1)} %heads.1) | copy-start | bytes 1572868
  6.7 0.9 %copy-start.5 = (bf16[512,128]{1,0:T(8,128)(2,1)S(1)}, bf16[512,128]{1,0:T(8,128)(2,1)}, u32[]{:S(2)}) copy-start(bf16[512,128]{1,0:T(8,128)(2,1)} %vfac.3) | copy-start | bytes 393220
  7.6 0.9 %copy-start.6 = (f32[256,256]{1,0:T(8,128)S(1)}, f32[256,256]{1,0:T(8,128)}, u32[]{:S(2)}) copy-start(f32[256,256]{1,0:T(8,128)} %omas.1) | copy-start | bytes 786436
  8.5 0.9 %copy-start.7 = (f32[128,256]{1,0:T(8,128)S(1)}, f32[128,256]{1,0:T(8,128)}, u32[]{:S(2)}) copy-start(f32[128,256]{1,0:T(8,128)} %vmas.1) | copy-start | bytes 393220
  9.4 0.8 %copy-start.8 = (f32[32,256]{1,0:T(8,128)S(1)}, f32[32,256]{1,0:T(8,128)}, u32[]{:S(2)}) copy-start(f32[32,256]{1,0:T(8,128)} %vm1.1) | copy-start | bytes 98308
  10.2 0.8 %copy-start.9 = (f32[32,256]{1,0:T(8,128)S(1)}, f32[32,256]{1,0:T(8,128)}, u32[]{:S(2)}) copy-start(f32[32,256]{1,0:T(8,128)} %vm2.1) | copy-start | bytes 98308
  11.0 0.8 %copy-start.10 = (f32[32,256]{1,0:T(8,128)S(1)}, f32[32,256]{1,0:T(8,128)}, u32[]{:S(2)}) copy-start(f32[32,256]{1,0:T(8,128)} %om1.1) | copy-start | bytes 98308
  11.7 0.8 %copy-start.11 = (f32[32,256]{1,0:T(8,128)S(1)}, f32[32,256]{1,0:T(8,128)}, u32[]{:S(2)}) copy-start(f32[32,256]{1,0:T(8,128)} %om2.1) | copy-start | bytes 98308

commit v2 on v1

--- a/solution.py
+++ b/solution.py
@@ -9,6 +9,7 @@
 
 MESH = pl.DeviceIdType.MESH
 ANY = pl.BlockSpec(memory_space=pl.ANY)
+HBM = pl.BlockSpec(memory_space=pltpu.HBM)
 VMEM = pl.BlockSpec(memory_space=pltpu.VMEM)
 BF16 = jnp.bfloat16
 F32 = jnp.float32
@@ -24,7 +25,7 @@
     fs, tp, pair,
     vin, vcot, vfac, vmas, vm1, vm2, heads, ocot, ofac, omas, om1, om2,
     v_all, o_all, v1_all, v2_all, o1_all, o2_all, vm_all, om_all, totals,
-    vin_v, vcot_v, heads_v, ocot_v, v1_v, v2_v, o1_v, o2_v, vm_v, om_v,
+    vfac_v, ofac_v, vin_v, vcot_v, heads_v, ocot_v, v1_v, v2_v, o1_v, o2_v, vm_v, om_v,
     heads_in, images, partial, partial_in, band_v, first_sums, second_sums,
     load_sem, own_sem, put_sem, heads_send, heads_recv, image_send, image_recv, relay_send,
     rs_send, rs_recv, all_send, all_recv, s1_send, s1_recv, s2_send, s2_recv, pre_send, pre_recv,
@@ -43,8 +44,8 @@
     def tp_peer(j):
         return lax.rem(t + j, tp)
 
-    sources = (heads, om1, om2, vm1, vm2, vcot, vin, omas, vmas, ocot)
-    places = (heads_v, o1_v, o2_v, v1_v, v2_v, vcot_v, vin_v, om_v, vm_v, ocot_v)
+    sources = (heads, om1, om2, vm1, vm2, vcot, vin, omas, vmas, ocot, vfac, ofac)
+    places = (heads_v, o1_v, o2_v, v1_v, v2_v, vcot_v, vin_v, om_v, vm_v, ocot_v, vfac_v, ofac_v)
     loads = [
         pltpu.make_async_copy(a, b, load_sem.at[i]) for i, (a, b) in enumerate(zip(sources, places))
     ]
@@ -106,11 +107,12 @@
 
     loads[5].wait()
     loads[6].wait()
+    loads[10].wait()
     total = jnp.zeros((2 * rank, columns), F32)
     step = 256 if tokens % 256 == 0 else tokens
     for i in range(tokens // step):
         rows = pl.ds(i * step, step)
-        image = jnp.dot(vcot_v[rows, :], vfac[...], preferred_element_type=F32)
+        image = jnp.dot(vcot_v[rows, :], vfac_v[...], preferred_element_type=F32)
         total = total + lax.dot_general(
             split(image, 1), vin_v[rows, :], (((0,), (0,)), ((), ())), preferred_element_type=F32
         )
@@ -163,10 +165,11 @@
     prefetch(5, loads[8], vm_v, vm_all)
 
     own_heads.wait()
+    loads[11].wait()
 
     def image_term(s):
         return jnp.dot(
-            heads_in[s], ofac[pl.ds(pl.multiple_of(s * width, width), width), :],
+            heads_in[s], ofac_v[pl.ds(pl.multiple_of(s * width, width), width), :],
             preferred_element_type=F32,
         )
 
@@ -315,10 +318,10 @@
             shape(fs * vmas.shape[0], columns), shape(fs * omas.shape[0], columns),
             shape(2, 8, 128),
         ),
-        in_specs=[ANY, ANY, VMEM, ANY, ANY, ANY, ANY, ANY, VMEM, ANY, ANY, ANY],
+        in_specs=[HBM] * 12,
         out_specs=(ANY,) * 8 + (VMEM,),
         scratch_shapes=[
-            like(vin), like(vcot), like(heads), like(ocot), like(vm1), like(vm2), like(om1), like(om2),
+            like(vfac), like(ofac), like(vin), like(vcot), like(heads), like(ocot), like(vm1), like(vm2), like(om1), like(om2),
             like(vmas), like(omas),
             pltpu.VMEM((tp, block, width), BF16),
             pltpu.VMEM((tp, rank, block), F32),
@@ -327,12 +330,12 @@
             pltpu.VMEM((2, band, columns), F32),
             pltpu.VMEM((2, fs, 8, 128), F32),
             pltpu.VMEM((2, tp, 8, 128), F32),
-            dma((10,)), dma, dma((8,)), dma((tp,)), dma((tp,)), dma((tp,)), dma((tp,)), dma((tp,)),
+            dma((12,)), dma, dma((8,)), dma((tp,)), dma((tp,)), dma((tp,)), dma((tp,)), dma((tp,)),
             dma((2, fs)), dma((2, fs)), dma((2, fs)), dma((2, fs)), dma((2, fs)), dma((2, fs)),
             dma((2, tp)), dma((2, tp)), dma((6, fs)), dma((6, fs)),
         ],
         compiler_params=pltpu.CompilerParams(
-            collective_id=0, has_side_effects=True, vmem_limit_bytes=40 * 1024 * 1024
+            collective_id=0, has_side_effects=True, vmem_limit_bytes=60 * 1024 * 1024
         ),
     )(vin, vcot, vfac, vmas, vm1, vm2, heads, ocot, ofac, omas, om1, om2)
     v_all, o_all, v1_all, v2_all, o1_all, o2_all, vm_all, om_all, totals = gathered
@@ -352,7 +355,7 @@
         ),
         in_specs=[VMEM] * 11,
         out_specs=(VMEM,) * 10,
-        compiler_params=pltpu.CompilerParams(vmem_limit_bytes=40 * 1024 * 1024),
+        compiler_params=pltpu.CompilerParams(vmem_limit_bytes=60 * 1024 * 1024),
     )(v_all, o_all, v1_all, v2_all, o1_all, o2_all, vm_all, om_all, totals, vfac, ofac)
 
 

time: 61 us -> 50.3 us (0.82)
  local copies, waits for them, and re-layouts: 11.8 us -> 0 us
  Pallas kernels: 47.8 us -> 49.5 us
    unnamed x24 -> x0, local copies, waits for them, and re-layouts: 11.8 us -> none
    pallas_call x1, Pallas kernels: 1.51 us -> 3.26 us  [on_device(): pl.pallas_call(functools.partial(finish_kernel, fs, tp), out_shape=(out(v...]
where the time goes in v2:
time: 50.3 us; the launch traced here: 50.1 us
  Pallas kernels  49.5 us (98%)
  between operations  0.65 us (1%)
    pallas_call x1, Pallas kernels, on_device(): pl.pallas_call(functools.partial(gather_kernel, fs, tp, pair), out_shape=...  46.2 us
    pallas_call x1, Pallas kernels, on_device(): pl.pallas_call(functools.partial(finish_kernel, fs, tp), out_shape=(out(v...  3.26 us

profile of v2, /device:TPU:0, one launch (start us, length us, event | category | flops | bytes accessed | tf_op | source)
XLA Modules:
  0.0 50.1 jit_solution(7196001077757040056)
XLA Ops:
  0.6 46.2 %shard_map.195 = (f32[4,32,256]{2,1,0:T(8,128)}, f32[4,32,256]{2,1,0:T(8,128)}, f32[128,256]{1,0:T(8,128)}, f32[128,256]{1,0:T(8,128)}, f32[128,256]{1,0:T(8,128...) custom-call(bf16[2048,256]{1,0:T(8,128)(2,1)} %vin.1, ...), custom_call_target="tpu_custom_call" | custom-call | tf_op jit(solution)/shard_map/pallas_call | solution.py:313
  46.9 3.3 %shard_map.196 = (f32[128,256]{1,0:T(8,128)}, f32[128,256]{1,0:T(8,128)}, bf16[512,256]{1,0:T(8,128)(2,1)}, f32[32,256]{1,0:T(8,128)}, f32[32,256]{1,0:T(8,128)}...) custom-call(f32[128,256]{1,0:T(8,128)} %bitcast.2, ...), custom_call_target="tpu_custom_call" | custom-call | tf_op jit(solution)/shard_map/pallas_call | solution.py:348
